TPU v7x, 32 devices: a whole 2x2x4 slice. The times are simulated.
32 devices in a mesh: ep: 32 (over z, y, x, core).
Axes of the slice: x: 2, y: 2, z: 4, core: 2. Of those that a mesh axis runs over, the one named last changes fastest.
Arguments:
- tokens: bfloat16 [8192, 2048], P('ep'), may hold values from -6 to 6
- norm_gain: float32 [2048], replicated, may hold values from 0.5 to 1.5
- expert_ids: int32 [8192, 2], P('ep'), may hold values from 0 to 31, all different within a row; in each aligned block of 256 rows (0 to 255, 256 to 511, ...) at most 48 rows name the same one
- route_scores: float32 [8192, 2], P('ep'), may hold values from -6 to 6
- gate_weight: bfloat16 [32, 2048, 1536], P('ep'), may hold values from -0.125 to 0.125
- up_weight: bfloat16 [32, 2048, 1536], P('ep'), may hold values from -0.125 to 0.125
- down_weight: bfloat16 [32, 1536, 2048], P('ep'), may hold values from -0.15625 to 0.15625
Outputs:
- mixed: bfloat16 [8192, 2048], P('ep')
Inputs may be any that keep to these rules, and one draw needn't show every extreme that they name: `expert_ids`: each row names 2 different experts. Among the 256 tokens of one device (each aligned block of 256 rows, in order) no expert is named by more than 48 tokens, a bound that some block reaches.
All inputs are finite; a program needn't handle non-finite values.
Results may differ from a plain program's by a relative error of at most 0.0025.
Values may be sent and summed in bfloat16 or wider, within the bound.
A program may use at most 128 MiB of HBM per device.

v0:
```python
import jax
import jax.numpy as jnp
from jax import lax
from jax.sharding import PartitionSpec as P

eps_norm = 1e-05


def expert_hidden(gate_pre, up_pre):
    return (jax.nn.silu(gate_pre) * up_pre).astype(jnp.bfloat16)


def on_device(tokens, norm_gain, expert_ids, route_scores, gate_weight, up_weight, down_weight):
    devices = lax.axis_size("ep")
    tok_count, top_count = expert_ids.shape
    model_width = tokens.shape[1]
    capacity = max(1, 3 * tok_count * top_count // devices)
    floats = tokens.astype(jnp.float32)
    scaled = floats * lax.rsqrt(jnp.mean(floats * floats, axis=-1, keepdims=True) + eps_norm)
    normed = (scaled * norm_gain).astype(jnp.bfloat16)
    flat_ids = expert_ids.reshape(-1)
    one_hot = (flat_ids[:, None] == jnp.arange(devices, dtype=jnp.int32)[None, :]).astype(jnp.int32)
    earlier = jnp.cumsum(one_hot, axis=0) - one_hot
    slot_rank = jnp.sum(earlier * one_hot, axis=1)
    position = flat_ids * capacity + slot_rank
    source_row = jnp.full((devices * capacity,), tok_count, jnp.int32)
    source_row = source_row.at[position].set(
        jnp.arange(tok_count * top_count, dtype=jnp.int32) // top_count
    )
    padded = jnp.concatenate([normed, jnp.zeros((1, model_width), jnp.bfloat16)], axis=0)
    send_rows = padded[source_row]
    gate_mat = gate_weight[0]
    up_mat = up_weight[0]
    down_mat = down_weight[0]
    arrived = lax.all_to_all(send_rows, "ep", split_axis=0, concat_axis=0, tiled=True)
    gate_pre = jnp.dot(arrived, gate_mat, preferred_element_type=jnp.float32)
    up_pre = jnp.dot(arrived, up_mat, preferred_element_type=jnp.float32)
    hidden = expert_hidden(gate_pre, up_pre)
    results = jnp.dot(hidden, down_mat, preferred_element_type=jnp.float32).astype(jnp.bfloat16)
    back_rows = lax.all_to_all(results, "ep", split_axis=0, concat_axis=0, tiled=True)
    picked = back_rows[position].reshape(tok_count, top_count, model_width).astype(jnp.float32)
    mix_weights = jax.nn.softmax(route_scores, axis=-1)
    return jnp.sum(mix_weights[:, :, None] * picked, axis=1).astype(jnp.bfloat16)


def solution(mesh):
    placed = (
        P("ep", None),
        P(),
        P("ep", None),
        P("ep", None),
        P("ep", None, None),
        P("ep", None, None),
        P("ep", None, None),
    )
    return jax.shard_map(
        on_device, mesh=mesh, in_specs=placed, out_specs=P("ep", None), check_vma=False
    )
```

profile of v0, /device:TPU:2, one launch (start us, length us, event | category | flops | bytes accessed | tf_op | source)
XLA Modules:
  0.0 373.8 jit_solution(15535027676914823244)
XLA Ops:
  0.0 0.8 copy.11
  0.8 0.1 eq.29
  1.0 0.1 eq.25
  1.1 0.7 broadcast_multiply_fusion
  1.8 1.2 reduce-window.6
  3.0 0.2 slice_reduce_fusion
  3.2 0.1 copy.10
  3.4 0.1 mul.61
  3.5 0.1 fusion.14
  3.7 2.5 scatter_custom_fusion
  6.1 1.5 fusion.9
  7.7 1.5 fusion.11
  9.2 0.1 concatenate.3
  9.3 7.1 %gather_fusion = bf16[1536,2048]{1,0:T(8,128)(2,1)} fusion(bf16[257,2048]{1,0:T(8,128)(2,1)S(1)} %concatenate.3, s32[2048]{0:T(1024)S(1)} %pad_clamp_fusion), kind=kCustom, calls=%fused_computation | custom fusion | bytes 12589056 | tf_op jit(solution)/shard_map/gather | solution.py:31
  16.4 146.3 %all_to_all.24 = bf16[32,48,2048]{2,1,0:T(8,128)(2,1)S(1)} all-to-all(bf16[32,48,2048]{2,1,0:T(8,128)(2,1)} %bitcast.37), channel_id=1, replica_groups=mesh['ep'=32] {'ep'}, dimensions={0} | all-to-all | bytes 12582912 | tf_op jit(solution)/shard_map/all_to_all | solution.py:35
  162.7 2.6 copy-done
  165.3 13.8 %fusion.6 = f32[1536,1536]{1,0:T(8,128)} fusion(bf16[1536,2048]{1,0:T(8,128)(2,1)S(1)} %bitcast.39, bf16[1,2048,1536]{2,1,0:T(8,128)(2,1)} %param.11), kind=kOutput, calls=%fused_computation.9 | convolution fusion | flops 9663676416 | bytes 22020096 | tf_op jit(solution)/shard_map/dot_general | solution.py:36
  179.1 28.8 %fusion.2 = bf16[1536,2048]{1,0:T(8,128)(2,1)} fusion(bf16[1536,2048]{1,0:T(8,128)(2,1)} %bitcast.40, f32[1536,1536]{1,0:T(8,128)} %fusion.6, bf16[1,1536,2048]{2,1,0:T(8,128)(2,1)} %param.13, bf16[1,2048,1536]{2,1,0:T(8,128)(2,1)} %param.12), kind=kOutput, calls=%fused_computation.6 | convolution fusion | flops 19344654336 | bytes 34603008 | tf_op jit(solution)/shard_map/dot_general | solution.py:39
  207.9 4.6 %all-to-all-start.1 = ((bf16[32,48,2048]{2,1,0:T(8,128)(2,1)}), bf16[32,48,2048]{2,1,0:T(8,128)(2,1)}, u32[]{:S(2)}, u32[]{:S(2)}) async-start(bf16[32,48,2048]{2,1,0:T(8,128)(2,1)} %bitcast.38), calls=%async_computation.1 | async-start | bytes 12582912 | tf_op jit(solution)/shard_map/all_to_all | solution.py:40
  212.5 0.1 copy.9
  212.7 139.2 %all-to-all-done.1 = bf16[32,48,2048]{2,1,0:T(8,128)(2,1)} async-done(((bf16[32,48,2048]{2,1,0:T(8,128)(2,1)}), bf16[32,48,2048]{2,1,0:T(8,128)(2,1)}, u32[]{:S(2)}, u32[]{:S(2)}) %all-to-all-start.1) | async-done | bytes 6291488 | tf_op jit(solution)/shard_map/all_to_all | solution.py:40
  351.9 8.0 %gather_fusion.1 = bf16[512,2048]{1,0:T(8,128)(2,1)S(1)} fusion(bf16[1536,2048]{1,0:T(8,128)(2,1)} %bitcast.9, s32[1024]{0:T(1024)S(1)} %pad_clamp_fusion.1), kind=kCustom, calls=%fused_computation.1 | custom fusion | bytes 4196352 | tf_op jit(solution)/shard_map/gather | solution.py:41
  359.9 4.0 %reshape.66 = f32[256,2,2048]{2,1,0:T(2,128)} reshape(bf16[512,2048]{1,0:T(8,128)(2,1)S(1)} %gather_fusion.1) | data formatting | bytes 6291456 | tf_op jit(solution)/shard_map/convert_element_type | solution.py:41
  363.9 9.9 %multiply_reduce_fusion = bf16[256,2048]{1,0:T(8,128)(2,1)} fusion(f32[256,2,2048]{2,1,0:T(2,128)} %reshape.66, f32[256,2]{1,0:T(8,128)S(1)} %copy.9), kind=kLoop, calls=%fused_computation.12 | loop fusion | flops 1572864 | bytes 5244928 | tf_op jit(solution)/shard_map/reduce_sum | solution.py:43
  (15 shorter events, 0.1 us)
Async XLA Ops:
  162.7 2.6 copy-start
  207.9 4.6 %copy-start.1 = (f32[256,2]{0,1:T(2,128)S(1)}, f32[256,2]{0,1:T(2,128)}, u32[]{:S(2)}) copy-start(f32[256,2]{0,1:T(2,128)} %param.10) | copy-start | bytes 6148
  207.9 144.1 %all-to-all-start.1 = ((bf16[32,48,2048]{2,1,0:T(8,128)(2,1)}), bf16[32,48,2048]{2,1,0:T(8,128)(2,1)}, u32[]{:S(2)}, u32[]{:S(2)}) async-start(bf16[32,48,2048]{2,1,0:T(8,128)(2,1)} %bitcast.38), calls=%async_computation.1 | async-start | bytes 12582912 | tf_op jit(solution)/shard_map/all_to_all | solution.py:40
where the time goes:
time: 374 us
  blocking collectives  146 us (39%)
  waiting for transfers between devices  139 us (37%)
  matrix products  42.5 us (11%)
  local copies, waits for them, and re-layouts  26 us (7%)
  other arithmetic  15 us (4%)
  starting transfers between devices  4.59 us (1%)
    all_to_all x1, blocking collectives, on_device(): lax.all_to_all(send_rows, 'ep', split_axis=0, concat_axis=0, tiled=True)  146 us
    all_to_all x1, waiting for transfers between devices, on_device(): lax.all_to_all(results, 'ep', split_axis=0, concat_axis=0, tiled=True)  139 us
    dot_general x1, matrix products, on_device(): jnp.dot(hidden, down_mat, preferred_element_type=jnp.float32)  28.8 us
    dot_general x1, matrix products, on_device(): gate_pre = jnp.dot(arrived, gate_mat, preferred_element_type=jnp.float32)  13.8 us
    reduce_sum x1, other arithmetic, on_device(): jnp.sum(mix_weights[:, :, None] * picked, axis=1).astype(jnp.bfloat16)  9.86 us
    gather x1, local copies, waits for them, and re-layouts, on_device(): back_rows[position].reshape(tok_count, top_count, model_width)  8 us
  transfers between devices with their start and end apart: 1, of which 1 were waited for; matrix products, arithmetic and copies ran while one was open for 0% of the time, Pallas kernels for 0%

commit v1 on v0

v1 whole, which is shorter than its diff:
```python
import jax
import jax.numpy as jnp
from jax import lax
from jax.sharding import PartitionSpec as P

eps_norm = 1e-05


def expert_hidden(gate_pre, up_pre):
    return (jax.nn.silu(gate_pre) * up_pre).astype(jnp.bfloat16)


def on_device(tokens, norm_gain, expert_ids, route_scores, gate_weight, up_weight, down_weight):
    devices = lax.axis_size("ep")
    half = devices // 2
    tok_count, top_count = expert_ids.shape
    capacity = max(1, 3 * tok_count * top_count // devices)
    slots = half * capacity
    me = lax.axis_index("ep")
    my_half = me // half
    across = [(i, (i + half) % devices) for i in range(devices)]
    groups = [list(range(half)), list(range(half, devices))]

    floats = tokens.astype(jnp.float32)
    scaled = floats * lax.rsqrt(jnp.mean(floats * floats, axis=-1, keepdims=True) + eps_norm)
    normed = (scaled * norm_gain).astype(jnp.bfloat16)
    far_normed = lax.ppermute(normed, "ep", across)

    flat_ids = expert_ids.reshape(-1)
    one_hot = (flat_ids[:, None] == jnp.arange(devices, dtype=jnp.int32)[None, :]).astype(jnp.int32)
    earlier = jnp.cumsum(one_hot, axis=0) - one_hot
    slot_rank = jnp.sum(earlier * one_hot, axis=1)
    position = (flat_ids * capacity + slot_rank).reshape(tok_count, top_count)
    mix_weights = jax.nn.softmax(route_scores, axis=-1)
    far_position = lax.ppermute(position, "ep", across)
    far_weights = lax.ppermute(mix_weights, "ep", across)

    gate_mat = gate_weight[0]
    up_mat = up_weight[0]
    down_mat = down_weight[0]

    near_at = position - my_half * slots
    far_at = far_position - my_half * slots

    def dispatch(rows, at):
        slot = jnp.arange(slots, dtype=jnp.int32)[:, None]
        chosen = slot == at[:, 0][None, :]
        for k in range(1, top_count):
            chosen = chosen | (slot == at[:, k][None, :])
        send = jnp.dot(
            chosen.astype(jnp.bfloat16), rows, preferred_element_type=jnp.float32
        ).astype(jnp.bfloat16)
        return lax.all_to_all(
            send, "ep", split_axis=0, concat_axis=0, tiled=True, axis_index_groups=groups
        )

    def experts(arrived):
        gate_pre = jnp.dot(arrived, gate_mat, preferred_element_type=jnp.float32)
        up_pre = jnp.dot(arrived, up_mat, preferred_element_type=jnp.float32)
        hidden = expert_hidden(gate_pre, up_pre)
        return jnp.dot(hidden, down_mat, preferred_element_type=jnp.float32).astype(jnp.bfloat16)

    def collect(results):
        return lax.all_to_all(
            results, "ep", split_axis=0, concat_axis=0, tiled=True, axis_index_groups=groups
        )

    def pick(back, at, k):
        slot = jnp.arange(slots, dtype=jnp.int32)[None, :]
        chosen = (slot == at[:, k][:, None]).astype(jnp.bfloat16)
        return jnp.dot(chosen, back, preferred_element_type=jnp.float32)

    near_arrived = dispatch(normed, near_at)
    far_arrived = dispatch(far_normed, far_at)
    far_back = collect(experts(far_arrived))
    near_back = collect(experts(near_arrived))

    far_in = (far_at >= 0) & (far_at < slots)
    far_all = jnp.all(far_in, axis=1, keepdims=True)
    far_coef = jnp.where(far_all, far_weights, far_in.astype(jnp.float32))
    reply = sum(far_coef[:, k][:, None] * pick(far_back, far_at, k) for k in range(top_count))
    reply = lax.ppermute(reply.astype(jnp.bfloat16), "ep", across)

    near_in = (near_at >= 0) & (near_at < slots)
    none_near = ~jnp.any(near_in, axis=1)
    reply_coef = jnp.sum(jnp.where(near_in, 0.0, mix_weights), axis=1)
    reply_coef = jnp.where(none_near, 1.0, reply_coef)
    total = sum(mix_weights[:, k][:, None] * pick(near_back, near_at, k) for k in range(top_count))
    return (total + reply_coef[:, None] * reply.astype(jnp.float32)).astype(jnp.bfloat16)


def solution(mesh):
    placed = (
        P("ep", None),
        P(),
        P("ep", None),
        P("ep", None),
        P("ep", None, None),
        P("ep", None, None),
        P("ep", None, None),
    )
    return jax.shard_map(
        on_device, mesh=mesh, in_specs=placed, out_specs=P("ep", None), check_vma=False
    )
```

time: 374 us -> 324 us (0.87)
  blocking collectives: 146 us -> 0 us
  waiting for transfers between devices: 139 us -> 213 us
  starting transfers between devices: 4.59 us -> 32.6 us
  matrix products: 42.5 us -> 68.4 us
  local copies, waits for them, and re-layouts: 26 us -> 4.3 us
  other arithmetic: 15 us -> 4.54 us
    all_to_all x1 -> x0, blocking collectives: 146 us -> none  [on_device(): lax.all_to_all(send_rows, 'ep', split_axis=0, concat_axis=0, tiled=True)]
    ppermute x0 -> x4, waiting for transfers between devices: none -> 130 us  [the longest x1 44.3 us: on_device(): reply = lax.ppermute(reply.astype(jnp.bfloat16), 'ep', across)]
    all_to_all x1 -> x4, waiting for transfers between devices: 139 us -> 82.8 us  [the longest x2 62.9 us: dispatch(): lax.all_to_all(send, 'ep', split_axis=0, concat_axis=0, tiled=True, axis_...]
    dot_general x2 -> x10, matrix products: 42.5 us -> 68.4 us  [the longest x2 34.4 us: experts(): jnp.dot(hidden, down_mat, preferred_element_type=jnp.float32)]
    all_to_all x1 -> x4, starting transfers between devices: 4.59 us -> 22.3 us  [the longest x2 11.5 us: collect(): lax.all_to_all(results, 'ep', split_axis=0, concat_axis=0, tiled=True, ax...]
    gather x2 -> x0, local copies, waits for them, and re-layouts: 15.1 us -> none  [the longest x1 8 us: on_device(): back_rows[position].reshape(tok_count, top_count, model_width)]
    ppermute x0 -> x4, starting transfers between devices: none -> 10.3 us  [the longest x1 3.83 us: on_device(): far_weights = lax.ppermute(mix_weights, 'ep', across)]
    reduce_sum x1, other arithmetic: 9.86 us -> 0.03 us  [on_device(): reply_coef = jnp.sum(jnp.where(near_in, 0.0, mix_weights), axis=1)]
  transfers between devices with their start and end apart: 1 -> 8, of which waited for: 1 -> 6; matrix products, arithmetic and copies ran while one was open for 0% -> 20% of each run, Pallas kernels for 0% -> 0%
where the time goes in v1:
time: 324 us; the launch traced here: 323 us
  waiting for transfers between devices  213 us (66%)
  matrix products  68.4 us (21%)
  starting transfers between devices  32.6 us (10%)
  other arithmetic  4.54 us (1%)
  local copies, waits for them, and re-layouts  4.3 us (1%)
    all_to_all x2, waiting for transfers between devices, dispatch(): lax.all_to_all(send, 'ep', split_axis=0, concat_axis=0, tiled=True, axis_...  62.9 us
    ppermute x1, waiting for transfers between devices, on_device(): reply = lax.ppermute(reply.astype(jnp.bfloat16), 'ep', across)  44.3 us
    ppermute x1, waiting for transfers between devices, on_device(): far_position = lax.ppermute(position, 'ep', across)  43.2 us
    ppermute x1, waiting for transfers between devices, on_device(): far_weights = lax.ppermute(mix_weights, 'ep', across)  42.9 us
    dot_general x2, matrix products, experts(): jnp.dot(hidden, down_mat, preferred_element_type=jnp.float32)  34.4 us
    all_to_all x2, waiting for transfers between devices, collect(): lax.all_to_all(results, 'ep', split_axis=0, concat_axis=0, tiled=True, ax...  19.9 us
    dot_general x2, matrix products, experts(): gate_pre = jnp.dot(arrived, gate_mat, preferred_element_type=jnp.float32)  19.1 us
    all_to_all x2, starting transfers between devices, collect(): lax.all_to_all(results, 'ep', split_axis=0, concat_axis=0, tiled=True, ax...  11.5 us
  transfers between devices with their start and end apart: 8, of which 6 were waited for; matrix products, arithmetic and copies ran while one was open for 20% of the time, Pallas kernels for 0%

profile of v1, /device:TPU:2, one launch (start us, length us, event | category | flops | bytes accessed | tf_op | source)
XLA Modules:
  0.0 323.3 jit_solution(16425150620492322530)
XLA Ops:
  3.1 2.7 collective-permute-start.2
  8.5 43.2 %collective-permute-done = s32[256,2]{0,1:T(2,128)S(1)} collective-permute-done((s32[256,2]{0,1:T(2,128)S(1)}, s32[256,2]{0,1:T(2,128)S(1)}, u32[]{:S(2)}, u32[]{:S(2)}) %collective-permute-start) | collective-permute-done | bytes 2080 | tf_op jit(solution)/shard_map/ppermute | solution.py:35
  51.8 2.7 convolution_convert_fusion
  54.4 4.7 %all-to-all-start.2 = ((bf16[16,48,2048]{2,1,0:T(8,128)(2,1)}), bf16[16,48,2048]{2,1,0:T(8,128)(2,1)}, u32[]{:S(2)}, u32[]{:S(2)}) async-start(bf16[16,48,2048]{2,1,0:T(8,128)(2,1)} %bitcast.15), calls=%async_computation.2 | async-start | bytes 6291456 | tf_op jit(solution)/shard_map/all_to_all | solution.py:53
  59.2 2.7 convolution_convert_fusion.1
  61.9 42.9 %all-to-all-done.2 = bf16[16,48,2048]{2,1,0:T(8,128)(2,1)} async-done(((bf16[16,48,2048]{2,1,0:T(8,128)(2,1)}), bf16[16,48,2048]{2,1,0:T(8,128)(2,1)}, u32[]{:S(2)}, u32[]{:S(2)}) %all-to-all-start.2) | async-done | bytes 3145760 | tf_op jit(solution)/shard_map/all_to_all | solution.py:53
  104.9 6.1 %all-to-all-start = ((bf16[16,48,2048]{2,1,0:T(8,128)(2,1)}), bf16[16,48,2048]{2,1,0:T(8,128)(2,1)S(1)}, u32[]{:S(2)}, u32[]{:S(2)}) async-start(bf16[16,48,2048]{2,1,0:T(8,128)(2,1)} %bitcast.4), calls=%async_computation | async-start | bytes 6291456 | tf_op jit(solution)/shard_map/all_to_all | solution.py:53
  110.9 9.5 %fusion.8 = f32[768,1536]{1,0:T(8,128)} fusion(bf16[768,2048]{1,0:T(8,128)(2,1)} %bitcast.16, bf16[1,2048,1536]{2,1,0:T(8,128)(2,1)} %param.11), kind=kOutput, calls=%fused_computation.8 | convolution fusion | flops 4831838208 | bytes 14155776 | tf_op jit(solution)/shard_map/dot_general | solution.py:58
  120.4 17.2 %fusion.19 = bf16[768,2048]{1,0:T(8,128)(2,1)} fusion(bf16[1,1536,2048]{2,1,0:T(8,128)(2,1)} %param.13, f32[768,1536]{1,0:T(8,128)} %fusion.8, bf16[768,2048]{1,0:T(8,128)(2,1)} %bitcast.16, bf16[1,2048,1536]{2,1,0:T(8,128)(2,1)} %param.12), kind=kOutput, calls=%fused_computation.17 | convolution fusion | flops 9672327168 | bytes 23592960 | tf_op jit(solution)/shard_map/dot_general | solution.py:61
  137.6 20.0 %all-to-all-done = bf16[16,48,2048]{2,1,0:T(8,128)(2,1)S(1)} async-done(((bf16[16,48,2048]{2,1,0:T(8,128)(2,1)}), bf16[16,48,2048]{2,1,0:T(8,128)(2,1)S(1)}, u32[]{:S(2)}, u32[]{:S(2)}) %all-to-all-start) | async-done | bytes 3145760 | tf_op jit(solution)/shard_map/all_to_all | solution.py:53
  157.6 1.7 copy-done.2
  159.4 5.7 %all-to-all-start.3 = ((bf16[16,48,2048]{2,1,0:T(8,128)(2,1)}), bf16[16,48,2048]{2,1,0:T(8,128)(2,1)S(1)}, u32[]{:S(2)}, u32[]{:S(2)}) async-start(bf16[16,48,2048]{2,1,0:T(8,128)(2,1)} %bitcast.79), calls=%async_computation.3 | async-start | bytes 6291456 | tf_op jit(solution)/shard_map/all_to_all | solution.py:64
  165.1 9.5 %fusion.10 = f32[768,1536]{1,0:T(8,128)} fusion(bf16[768,2048]{1,0:T(8,128)(2,1)} %bitcast.77, bf16[1,2048,1536]{2,1,0:T(8,128)(2,1)} %param.11), kind=kOutput, calls=%fused_computation.10 | convolution fusion | flops 4831838208 | bytes 14155776 | tf_op jit(solution)/shard_map/dot_general | solution.py:58
  174.6 17.2 %fusion.16 = bf16[768,2048]{1,0:T(8,128)(2,1)} fusion(bf16[1,1536,2048]{2,1,0:T(8,128)(2,1)} %param.13, f32[768,1536]{1,0:T(8,128)} %fusion.10, bf16[768,2048]{1,0:T(8,128)(2,1)} %bitcast.78, bf16[1,2048,1536]{2,1,0:T(8,128)(2,1)} %param.12), kind=kOutput, calls=%fused_computation.16 | convolution fusion | flops 9672327168 | bytes 23592960 | tf_op jit(solution)/shard_map/dot_general | solution.py:61
  191.8 19.9 %all-to-all-done.3 = bf16[16,48,2048]{2,1,0:T(8,128)(2,1)S(1)} async-done(((bf16[16,48,2048]{2,1,0:T(8,128)(2,1)}), bf16[16,48,2048]{2,1,0:T(8,128)(2,1)S(1)}, u32[]{:S(2)}, u32[]{:S(2)}) %all-to-all-start.3) | async-done | bytes 3145760 | tf_op jit(solution)/shard_map/all_to_all | solution.py:64
  211.7 1.7 copy-done
  213.4 5.8 %all-to-all-start.1 = ((bf16[16,48,2048]{2,1,0:T(8,128)(2,1)}), bf16[16,48,2048]{2,1,0:T(8,128)(2,1)S(1)}, u32[]{:S(2)}, u32[]{:S(2)}) async-start(bf16[16,48,2048]{2,1,0:T(8,128)(2,1)} %bitcast.76), calls=%async_computation.1 | async-start | bytes 6291456 | tf_op jit(solution)/shard_map/all_to_all | solution.py:64
  219.2 3.8 %collective-permute-start.1 = (f32[256,2]{0,1:T(2,128)S(1)}, f32[256,2]{0,1:T(2,128)S(1)}, u32[]{:S(2)}, u32[]{:S(2)}) collective-permute-start(f32[256,2]{0,1:T(2,128)S(1)} %get-tuple-element.6), channel_id=1, source_target_pairs={{0,16},{1,17},{2,18},{3,19},{4,20},{5,21},{6,22},{7,23},{8,24},{9,... | collective-permute-start | bytes 6152 | tf_op jit(solution)/shard_map/ppermute | solution.py:36
  223.0 42.9 %collective-permute-done.1 = f32[256,2]{0,1:T(2,128)S(1)} collective-permute-done((f32[256,2]{0,1:T(2,128)S(1)}, f32[256,2]{0,1:T(2,128)S(1)}, u32[]{:S(2)}, u32[]{:S(2)}) %collective-permute-start.1) | collective-permute-done | bytes 2080 | tf_op jit(solution)/shard_map/ppermute | solution.py:36
  266.0 2.9 fusion.35
  268.9 2.2 add_convert_fusion.1
  271.1 3.4 %collective-permute-start.3 = (bf16[256,2048]{1,0:T(8,128)(2,1)}, bf16[256,2048]{1,0:T(8,128)(2,1)}, u32[]{:S(2)}, u32[]{:S(2)}) collective-permute-start(bf16[256,2048]{1,0:T(8,128)(2,1)} %add_convert_fusion.1), channel_id=1, source_target_pairs={{0,16},{1,17},{2,18},{3,19},{4,20},{5,21},{6,22},{7,23},{8,24},{9,... | collective-permute-start | bytes 3145736 | tf_op jit(solution)/shard_map/ppermute | solution.py:82
  275.5 44.3 %collective-permute-done.3 = bf16[256,2048]{1,0:T(8,128)(2,1)} collective-permute-done((bf16[256,2048]{1,0:T(8,128)(2,1)}, bf16[256,2048]{1,0:T(8,128)(2,1)}, u32[]{:S(2)}, u32[]{:S(2)}) %collective-permute-start.3) | collective-permute-done | bytes 1048608 | tf_op jit(solution)/shard_map/ppermute | solution.py:82
  319.9 3.4 %add_convert_fusion = bf16[256,2048]{1,0:T(8,128)(2,1)} fusion(bf16[256,2048]{1,0:T(8,128)(2,1)} %collective-permute-done.3, f32[256]{0:T(256)S(1)} %broadcast_select_fusion, f32[256,2048]{1,0:T(8,128)S(1)} %convolution_multiply_fusion.1, bf16[768,2048]{1,0:T(8,128)(2,1)S(1)} %bitcast.73, s32[256]{0:T(256)S(1)} %bitcast.81, f32[256]{0:T(256)S(1)} %bitcast.84), kind=kOutput, calls=%fused_computation.26 | convolution fusion | flops 808648704 | bytes 7343104 | tf_op jit(solution)/shard_map/dot_general | solution.py:71
  (37 shorter events, 6.9 us)
Async XLA Ops:
  0.0 5.7 %copy-start.4 = (s32[256,2]{0,1:T(2,128)S(1)}, s32[256,2]{0,1:T(2,128)}, u32[]{:S(2)}) copy-start(s32[256,2]{0,1:T(2,128)} %param.9) | copy-start | bytes 6148
  0.0 8.0 %copy-start.3 = (f32[256,2]{0,1:T(2,128)S(1)}, f32[256,2]{0,1:T(2,128)}, u32[]{:S(2)}) copy-start(f32[256,2]{0,1:T(2,128)} %param.10) | copy-start | bytes 6148
  3.1 48.7 %collective-permute-start.2 = (bf16[256,2048]{1,0:T(8,128)(2,1)S(1)}, bf16[256,2048]{1,0:T(8,128)(2,1)S(1)}, u32[]{:S(2)}, u32[]{:S(2)}) collective-permute-start(bf16[256,2048]{1,0:T(8,128)(2,1)S(1)} %fusion.25), channel_id=1, source_target_pairs={{0,16},{1,17},{2,18},{3,19},{4,20},{5,21},{6,22},{7,23},{8,24},{9,... | collective-permute-start | bytes 3145736 | tf_op jit(solution)/shard_map/ppermute | solution.py:27
  8.1 43.6 %collective-permute-start = (s32[256,2]{0,1:T(2,128)S(1)}, s32[256,2]{0,1:T(2,128)S(1)}, u32[]{:S(2)}, u32[]{:S(2)}) collective-permute-start(s32[256,2]{0,1:T(2,128)S(1)} %get-tuple-element.8), channel_id=1, source_target_pairs={{0,16},{1,17},{2,18},{3,19},{4,20},{5,21},{6,22},{7,23},{8,24},{9,... | collective-permute-start | bytes 6152 | tf_op jit(solution)/shard_map/ppermute | solution.py:35
  54.4 50.4 %all-to-all-start.2 = ((bf16[16,48,2048]{2,1,0:T(8,128)(2,1)}), bf16[16,48,2048]{2,1,0:T(8,128)(2,1)}, u32[]{:S(2)}, u32[]{:S(2)}) async-start(bf16[16,48,2048]{2,1,0:T(8,128)(2,1)} %bitcast.15), calls=%async_computation.2 | async-start | bytes 6291456 | tf_op jit(solution)/shard_map/all_to_all | solution.py:53
  104.9 52.8 %all-to-all-start = ((bf16[16,48,2048]{2,1,0:T(8,128)(2,1)}), bf16[16,48,2048]{2,1,0:T(8,128)(2,1)S(1)}, u32[]{:S(2)}, u32[]{:S(2)}) async-start(bf16[16,48,2048]{2,1,0:T(8,128)(2,1)} %bitcast.4), calls=%async_computation | async-start | bytes 6291456 | tf_op jit(solution)/shard_map/all_to_all | solution.py:53
  157.6 1.8 copy-start.2
  159.4 52.3 %all-to-all-start.3 = ((bf16[16,48,2048]{2,1,0:T(8,128)(2,1)}), bf16[16,48,2048]{2,1,0:T(8,128)(2,1)S(1)}, u32[]{:S(2)}, u32[]{:S(2)}) async-start(bf16[16,48,2048]{2,1,0:T(8,128)(2,1)} %bitcast.79), calls=%async_computation.3 | async-start | bytes 6291456 | tf_op jit(solution)/shard_map/all_to_all | solution.py:64
  211.7 1.7 copy-start
  213.4 61.1 %all-to-all-start.1 = ((bf16[16,48,2048]{2,1,0:T(8,128)(2,1)}), bf16[16,48,2048]{2,1,0:T(8,128)(2,1)S(1)}, u32[]{:S(2)}, u32[]{:S(2)}) async-start(bf16[16,48,2048]{2,1,0:T(8,128)(2,1)} %bitcast.76), calls=%async_computation.1 | async-start | bytes 6291456 | tf_op jit(solution)/shard_map/all_to_all | solution.py:64
  219.2 49.7 %copy-start.1 = (bf16[16,48,2048]{2,1,0:T(8,128)(2,1)S(1)}, bf16[16,48,2048]{2,1,0:T(8,128)(2,1)}, u32[]{:S(2)}) copy-start(bf16[16,48,2048]{2,1,0:T(8,128)(2,1)} %copy-done) | copy-start | bytes 9437188
  219.2 46.8 %collective-permute-start.1 = (f32[256,2]{0,1:T(2,128)S(1)}, f32[256,2]{0,1:T(2,128)S(1)}, u32[]{:S(2)}, u32[]{:S(2)}) collective-permute-start(f32[256,2]{0,1:T(2,128)S(1)} %get-tuple-element.6), channel_id=1, source_target_pairs={{0,16},{1,17},{2,18},{3,19},{4,20},{5,21},{6,22},{7,23},{8,24},{9,... | collective-permute-start | bytes 6152 | tf_op jit(solution)/shard_map/ppermute | solution.py:36
  271.1 48.8 %collective-permute-start.3 = (bf16[256,2048]{1,0:T(8,128)(2,1)}, bf16[256,2048]{1,0:T(8,128)(2,1)}, u32[]{:S(2)}, u32[]{:S(2)}) collective-permute-start(bf16[256,2048]{1,0:T(8,128)(2,1)} %add_convert_fusion.1), channel_id=1, source_target_pairs={{0,16},{1,17},{2,18},{3,19},{4,20},{5,21},{6,22},{7,23},{8,24},{9,... | collective-permute-start | bytes 3145736 | tf_op jit(solution)/shard_map/ppermute | solution.py:82

commit v2 on v1

--- a/solution.py
+++ b/solution.py
@@ -32,15 +32,14 @@
     slot_rank = jnp.sum(earlier * one_hot, axis=1)
     position = (flat_ids * capacity + slot_rank).reshape(tok_count, top_count)
     mix_weights = jax.nn.softmax(route_scores, axis=-1)
-    far_position = lax.ppermute(position, "ep", across)
-    far_weights = lax.ppermute(mix_weights, "ep", across)
+    plan = jnp.concatenate([position.astype(jnp.float32), mix_weights], axis=1)
+    far_plan = lax.ppermute(plan, "ep", across)
 
     gate_mat = gate_weight[0]
     up_mat = up_weight[0]
     down_mat = down_weight[0]
 
     near_at = position - my_half * slots
-    far_at = far_position - my_half * slots
 
     def dispatch(rows, at):
         slot = jnp.arange(slots, dtype=jnp.int32)[:, None]
@@ -71,9 +70,16 @@
         return jnp.dot(chosen, back, preferred_element_type=jnp.float32)
 
     near_arrived = dispatch(normed, near_at)
+    near_arrived, far_normed, far_plan = lax.optimization_barrier((near_arrived, far_normed, far_plan))
+    far_position = far_plan[:, :top_count].astype(jnp.int32)
+    far_weights = far_plan[:, top_count:]
+    far_at = far_position - my_half * slots
     far_arrived = dispatch(far_normed, far_at)
+    near_results = experts(near_arrived)
+    far_arrived, near_results = lax.optimization_barrier((far_arrived, near_results))
     far_back = collect(experts(far_arrived))
-    near_back = collect(experts(near_arrived))
+    far_back, near_results = lax.optimization_barrier((far_back, near_results))
+    near_back = collect(near_results)
 
     far_in = (far_at >= 0) & (far_at < slots)
     far_all = jnp.all(far_in, axis=1, keepdims=True)

time: 324 us -> 291 us (0.90)
  waiting for transfers between devices: 213 us -> 146 us
  blocking collectives: 0 us -> 41.2 us
  starting transfers between devices: 32.6 us -> 23.6 us
    all_to_all x2, waiting for transfers between devices: 62.9 us -> 19.8 us  [dispatch(): lax.all_to_all(send, 'ep', split_axis=0, concat_axis=0, tiled=True, axis_...]
    all_to_all x0 -> x1, blocking collectives: none -> 41.2 us  [collect(): lax.all_to_all(results, 'ep', split_axis=0, concat_axis=0, tiled=True, ax...]
    ppermute x1, waiting for transfers between devices: 44.3 us -> 11.5 us  [on_device(): reply = lax.ppermute(reply.astype(jnp.bfloat16), 'ep', across)]
    all_to_all x2 -> x1, waiting for transfers between devices: 19.9 us -> 48.8 us  [collect(): lax.all_to_all(results, 'ep', split_axis=0, concat_axis=0, tiled=True, ax...]
    ppermute x2 -> x1, waiting for transfers between devices: 86.2 us -> 66.1 us  [on_device(): far_plan = lax.ppermute(plan, 'ep', across)]
    dot_general x2 -> x1, matrix products: 19.1 us -> 9.38 us  [experts(): gate_pre = jnp.dot(arrived, gate_mat, preferred_element_type=jnp.float32)]
    dot_general x0 -> x1, matrix products: none -> 9.52 us  [experts(): up_pre = jnp.dot(arrived, up_mat, preferred_element_type=jnp.float32)]
    ppermute x2 -> x1, starting transfers between devices: 4.23 us -> 0.4 us  [on_device(): far_plan = lax.ppermute(plan, 'ep', across)]
  transfers between devices with their start and end apart: 8 -> 6, of which waited for: 6 -> 4; matrix products, arithmetic and copies ran while one was open for 20% -> 11% of each run, Pallas kernels for 0% -> 0%
where the time goes in v2:
time: 291 us; the launch traced here: 289 us
  waiting for transfers between devices  146 us (50%)
  matrix products  69.9 us (24%)
  blocking collectives  41.2 us (14%)
  starting transfers between devices  23.6 us (8%)
  other arithmetic  6.58 us (2%)
    ppermute x1, waiting for transfers between devices, on_device(): far_plan = lax.ppermute(plan, 'ep', across)  66.1 us
    all_to_all x1, waiting for transfers between devices, collect(): lax.all_to_all(results, 'ep', split_axis=0, concat_axis=0, tiled=True, ax...  48.8 us
    all_to_all x1, blocking collectives, collect(): lax.all_to_all(results, 'ep', split_axis=0, concat_axis=0, tiled=True, ax...  41.2 us
    dot_general x2, matrix products, experts(): jnp.dot(hidden, down_mat, preferred_element_type=jnp.float32)  35.3 us
    all_to_all x2, waiting for transfers between devices, dispatch(): lax.all_to_all(send, 'ep', split_axis=0, concat_axis=0, tiled=True, axis_...  19.8 us
    ppermute x1, waiting for transfers between devices, on_device(): reply = lax.ppermute(reply.astype(jnp.bfloat16), 'ep', across)  11.5 us
    dot_general x4, matrix products, pick(): return jnp.dot(chosen, back, preferred_element_type=jnp.float32)  10.3 us
    all_to_all x2, starting transfers between devices, dispatch(): lax.all_to_all(send, 'ep', split_axis=0, concat_axis=0, tiled=True, axis_...  10.3 us
  transfers between devices with their start and end apart: 6, of which 4 were waited for; matrix products, arithmetic and copies ran while one was open for 11% of the time, Pallas kernels for 0%

profile of v2, /device:TPU:2, one launch (start us, length us, event | category | flops | bytes accessed | tf_op | source)
XLA Modules:
  0.0 289.2 jit_solution(4944455884901532424)
XLA Ops:
  0.0 0.8 copy.43
  2.5 1.5 fusion.24
  4.1 1.2 reduce-window.6
  6.6 1.5 fusion.26
  8.1 2.7 convolution_convert_fusion.1
  10.8 5.4 %all-to-all-start = ((bf16[16,48,2048]{2,1,0:T(8,128)(2,1)}), bf16[16,48,2048]{2,1,0:T(8,128)(2,1)}, u32[]{:S(2)}, u32[]{:S(2)}) async-start(bf16[16,48,2048]{2,1,0:T(8,128)(2,1)} %bitcast.4), calls=%async_computation | async-start | bytes 6291456 | tf_op jit(solution)/shard_map/all_to_all | solution.py:52
  16.2 2.6 collective-permute-start
  19.2 66.1 %collective-permute-done.1 = f32[256,4]{0,1:T(4,128)S(1)} collective-permute-done((f32[256,4]{0,1:T(4,128)S(1)}, f32[256,4]{0,1:T(4,128)S(1)}, u32[]{:S(2)}, u32[]{:S(2)}) %collective-permute-start.1) | collective-permute-done | bytes 4128 | tf_op jit(solution)/shard_map/ppermute | solution.py:36
  85.4 2.7 convolution_convert_fusion
  88.1 4.8 %all-to-all-start.1 = ((bf16[16,48,2048]{2,1,0:T(8,128)(2,1)}), bf16[16,48,2048]{2,1,0:T(8,128)(2,1)S(1)}, u32[]{:S(2)}, u32[]{:S(2)}) async-start(bf16[16,48,2048]{2,1,0:T(8,128)(2,1)} %bitcast.8), calls=%async_computation.1 | async-start | bytes 6291456 | tf_op jit(solution)/shard_map/all_to_all | solution.py:52
  93.0 9.5 %fusion.6 = f32[768,1536]{1,0:T(8,128)} fusion(bf16[768,2048]{1,0:T(8,128)(2,1)} %bitcast.5, bf16[1,2048,1536]{2,1,0:T(8,128)(2,1)} %param.12), kind=kOutput, calls=%fused_computation.6 | convolution fusion | flops 4831838208 | bytes 14155776 | tf_op jit(solution)/shard_map/dot_general | solution.py:58
  102.5 17.4 %fusion.14 = bf16[768,2048]{1,0:T(8,128)(2,1)} fusion(bf16[1,1536,2048]{2,1,0:T(8,128)(2,1)} %param.13, f32[768,1536]{1,0:T(8,128)} %fusion.6, bf16[768,2048]{1,0:T(8,128)(2,1)} %bitcast.5, bf16[1,2048,1536]{2,1,0:T(8,128)(2,1)} %param.11), kind=kOutput, calls=%fused_computation.16 | convolution fusion | flops 9672327168 | bytes 23592960 | tf_op jit(solution)/shard_map/dot_general | solution.py:60
  119.9 19.8 %all-to-all-done.1 = bf16[16,48,2048]{2,1,0:T(8,128)(2,1)S(1)} async-done(((bf16[16,48,2048]{2,1,0:T(8,128)(2,1)}), bf16[16,48,2048]{2,1,0:T(8,128)(2,1)S(1)}, u32[]{:S(2)}, u32[]{:S(2)}) %all-to-all-start.1) | async-done | bytes 3145760 | tf_op jit(solution)/shard_map/all_to_all | solution.py:52
  139.7 9.4 %fusion.8 = f32[768,1536]{1,0:T(8,128)} fusion(bf16[768,2048]{1,0:T(8,128)(2,1)S(1)} %bitcast.75, bf16[1,2048,1536]{2,1,0:T(8,128)(2,1)} %param.11), kind=kOutput, calls=%fused_computation.8 | convolution fusion | flops 4831838208 | bytes 14155776 | tf_op jit(solution)/shard_map/dot_general | solution.py:57
  149.0 17.9 %fusion.17 = bf16[768,2048]{1,0:T(8,128)(2,1)} fusion(bf16[1,1536,2048]{2,1,0:T(8,128)(2,1)} %param.13, f32[768,1536]{1,0:T(8,128)} %fusion.8, bf16[768,2048]{1,0:T(8,128)(2,1)S(1)} %bitcast.76, bf16[1,2048,1536]{2,1,0:T(8,128)(2,1)} %param.12), kind=kOutput, calls=%fused_computation.17 | convolution fusion | flops 9672327168 | bytes 23592960 | tf_op jit(solution)/shard_map/dot_general | solution.py:60
  166.9 41.2 %all_to_all.48 = bf16[16,48,2048]{2,1,0:T(8,128)(2,1)S(1)} all-to-all(bf16[16,48,2048]{2,1,0:T(8,128)(2,1)} %bitcast.77), channel_id=1, replica_groups={{0,1,2,3,4,5,6,7,8,9,10,11,12,13,14,15},{16,17,18,19,20,21,22,23,24,25,..., dimensions={0} | all-to-all | bytes 6291456 | tf_op jit(solution)/shard_map/all_to_all | solution.py:63
  208.2 8.0 %all-to-all-start.3 = ((bf16[16,48,2048]{2,1,0:T(8,128)(2,1)}), bf16[16,48,2048]{2,1,0:T(8,128)(2,1)}, u32[]{:S(2)}, u32[]{:S(2)}) async-start(bf16[16,48,2048]{2,1,0:T(8,128)(2,1)} %bitcast.74), calls=%async_computation.3 | async-start | bytes 6291456 | tf_op jit(solution)/shard_map/all_to_all | solution.py:63
  216.2 1.1 convolution_multiply_fusion.1
  217.3 2.1 fusion.22
  219.4 2.4 collective-permute-start.2
  221.8 48.8 %all-to-all-done.3 = bf16[16,48,2048]{2,1,0:T(8,128)(2,1)} async-done(((bf16[16,48,2048]{2,1,0:T(8,128)(2,1)}), bf16[16,48,2048]{2,1,0:T(8,128)(2,1)}, u32[]{:S(2)}, u32[]{:S(2)}) %all-to-all-start.3) | async-done | bytes 3145760 | tf_op jit(solution)/shard_map/all_to_all | solution.py:63
  270.6 2.9 %convolution_multiply_fusion.3 = f32[256,2048]{1,0:T(8,128)S(1)} fusion(bf16[768,2048]{1,0:T(8,128)(2,1)} %bitcast.16, f32[256]{0:T(256)S(1)} %bitcast.88, s32[256]{0:T(256)S(1)} %bitcast.85), kind=kOutput, calls=%fused_computation.23 | convolution fusion | flops 806027264 | bytes 5244928 | tf_op jit(solution)/shard_map/dot_general | solution.py:70
  273.5 11.5 %collective-permute-done.2 = bf16[256,2048]{1,0:T(8,128)(2,1)S(1)} collective-permute-done((bf16[256,2048]{1,0:T(8,128)(2,1)}, bf16[256,2048]{1,0:T(8,128)(2,1)S(1)}, u32[]{:S(2)}, u32[]{:S(2)}) %collective-permute-start.2) | collective-permute-done | bytes 1048608 | tf_op jit(solution)/shard_map/ppermute | solution.py:88
  285.0 4.2 %add_convert_fusion = bf16[256,2048]{1,0:T(8,128)(2,1)} fusion(bf16[256,2048]{1,0:T(8,128)(2,1)S(1)} %collective-permute-done.2, f32[256]{0:T(256)S(1)} %broadcast_select_fusion, f32[256,2048]{1,0:T(8,128)S(1)} %convolution_multiply_fusion.3, bf16[768,2048]{1,0:T(8,128)(2,1)} %bitcast.16, f32[256]{0:T(256)S(1)} %bitcast.82, s32[256]{0:T(256)S(1)} %bitcast.79), kind=kOutput, calls=%fused_computation.31 | convolution fusion | flops 808648704 | bytes 7343104 | tf_op jit(solution)/shard_map/dot_general | solution.py:70
  (28 shorter events, 3.5 us)
Async XLA Ops:
  10.8 8.0 %copy-start = (s32[256,2]{0,1:T(2,128)S(1)}, s32[256,2]{0,1:T(2,128)}, u32[]{:S(2)}) copy-start(s32[256,2]{0,1:T(2,128)} %param.9) | copy-start | bytes 6148
  10.8 74.6 %all-to-all-start = ((bf16[16,48,2048]{2,1,0:T(8,128)(2,1)}), bf16[16,48,2048]{2,1,0:T(8,128)(2,1)}, u32[]{:S(2)}, u32[]{:S(2)}) async-start(bf16[16,48,2048]{2,1,0:T(8,128)(2,1)} %bitcast.4), calls=%async_computation | async-start | bytes 6291456 | tf_op jit(solution)/shard_map/all_to_all | solution.py:52
  16.2 69.2 %collective-permute-start = (bf16[256,2048]{1,0:T(8,128)(2,1)S(1)}, bf16[256,2048]{1,0:T(8,128)(2,1)S(1)}, u32[]{:S(2)}, u32[]{:S(2)}) collective-permute-start(bf16[256,2048]{1,0:T(8,128)(2,1)S(1)} %fusion.26), channel_id=1, source_target_pairs={{0,16},{1,17},{2,18},{3,19},{4,20},{5,21},{6,22},{7,23},{8,24},{9,... | collective-permute-start | bytes 3145736 | tf_op jit(solution)/shard_map/ppermute | solution.py:27
  18.8 66.5 %collective-permute-start.1 = (f32[256,4]{0,1:T(4,128)S(1)}, f32[256,4]{0,1:T(4,128)S(1)}, u32[]{:S(2)}, u32[]{:S(2)}) collective-permute-start(f32[256,4]{0,1:T(4,128)S(1)} %pad_maximum_fusion), channel_id=1, source_target_pairs={{0,16},{1,17},{2,18},{3,19},{4,20},{5,21},{6,22},{7,23},{8,24},{9,... | collective-permute-start | bytes 12296 | tf_op jit(solution)/shard_map/ppermute | solution.py:36
  88.1 51.5 %all-to-all-start.1 = ((bf16[16,48,2048]{2,1,0:T(8,128)(2,1)}), bf16[16,48,2048]{2,1,0:T(8,128)(2,1)S(1)}, u32[]{:S(2)}, u32[]{:S(2)}) async-start(bf16[16,48,2048]{2,1,0:T(8,128)(2,1)} %bitcast.8), calls=%async_computation.1 | async-start | bytes 6291456 | tf_op jit(solution)/shard_map/all_to_all | solution.py:52
  208.2 62.4 %all-to-all-start.3 = ((bf16[16,48,2048]{2,1,0:T(8,128)(2,1)}), bf16[16,48,2048]{2,1,0:T(8,128)(2,1)}, u32[]{:S(2)}, u32[]{:S(2)}) async-start(bf16[16,48,2048]{2,1,0:T(8,128)(2,1)} %bitcast.74), calls=%async_computation.3 | async-start | bytes 6291456 | tf_op jit(solution)/shard_map/all_to_all | solution.py:63
  219.4 65.6 %collective-permute-start.2 = (bf16[256,2048]{1,0:T(8,128)(2,1)}, bf16[256,2048]{1,0:T(8,128)(2,1)S(1)}, u32[]{:S(2)}, u32[]{:S(2)}) collective-permute-start(bf16[256,2048]{1,0:T(8,128)(2,1)} %fusion.22), channel_id=1, source_target_pairs={{0,16},{1,17},{2,18},{3,19},{4,20},{5,21},{6,22},{7,23},{8,24},{9,... | collective-permute-start | bytes 3145736 | tf_op jit(solution)/shard_map/ppermute | solution.py:88

commit v3 on v2

--- a/solution.py
+++ b/solution.py
@@ -41,8 +41,9 @@
 
     near_at = position - my_half * slots
 
-    def dispatch(rows, at):
-        slot = jnp.arange(slots, dtype=jnp.int32)[:, None]
+    def dispatch(rows, at, first, last):
+        own = jnp.arange(half, dtype=jnp.int32)[:, None] * capacity
+        slot = (own + jnp.arange(first, last, dtype=jnp.int32)[None, :]).reshape(-1, 1)
         chosen = slot == at[:, 0][None, :]
         for k in range(1, top_count):
             chosen = chosen | (slot == at[:, k][None, :])
@@ -69,15 +70,23 @@
         chosen = (slot == at[:, k][:, None]).astype(jnp.bfloat16)
         return jnp.dot(chosen, back, preferred_element_type=jnp.float32)
 
-    near_arrived = dispatch(normed, near_at)
-    near_arrived, far_normed, far_plan = lax.optimization_barrier((near_arrived, far_normed, far_plan))
+    cut = capacity // 2
+    early_arrived = dispatch(normed, near_at, 0, cut)
+    early_arrived, far_normed, far_plan = lax.optimization_barrier((early_arrived, far_normed, far_plan))
     far_position = far_plan[:, :top_count].astype(jnp.int32)
     far_weights = far_plan[:, top_count:]
     far_at = far_position - my_half * slots
-    far_arrived = dispatch(far_normed, far_at)
-    near_results = experts(near_arrived)
-    far_arrived, near_results = lax.optimization_barrier((far_arrived, near_results))
-    far_back = collect(experts(far_arrived))
+    far_arrived = dispatch(far_normed, far_at, 0, capacity)
+    early_results = experts(early_arrived)
+    far_arrived, early_results, near_rows = lax.optimization_barrier((far_arrived, early_results, normed))
+    late_arrived = dispatch(near_rows, near_at, cut, capacity)
+    far_results = experts(far_arrived)
+    far_results, late_arrived = lax.optimization_barrier((far_results, late_arrived))
+    far_back = collect(far_results)
+    late_results = experts(late_arrived)
+    near_results = jnp.concatenate(
+        [early_results.reshape(half, cut, -1), late_results.reshape(half, capacity - cut, -1)], axis=1
+    ).reshape(slots, -1)
     far_back, near_results = lax.optimization_barrier((far_back, near_results))
     near_back = collect(near_results)
 

time: 291 us -> 286 us (0.983)
  blocking collectives: 41.2 us -> 0 us
  matrix products: 69.9 us -> 81.8 us
  starting transfers between devices: 23.6 us -> 33.6 us
  waiting for transfers between devices: 146 us -> 155 us
  other arithmetic: 6.58 us -> 10.2 us
    all_to_all x1 -> x0, blocking collectives: 41.2 us -> none  [collect(): lax.all_to_all(results, 'ep', split_axis=0, concat_axis=0, tiled=True, ax...]
    all_to_all x1 -> x2, waiting for transfers between devices: 48.8 us -> 70.8 us  [collect(): lax.all_to_all(results, 'ep', split_axis=0, concat_axis=0, tiled=True, ax...]
    ppermute x1, waiting for transfers between devices: 66.1 us -> 46 us  [on_device(): far_plan = lax.ppermute(plan, 'ep', across)]
    dot_general x1 -> x2, matrix products: 9.38 us -> 16.8 us  [experts(): gate_pre = jnp.dot(arrived, gate_mat, preferred_element_type=jnp.float32)]
    all_to_all x2 -> x3, waiting for transfers between devices: 19.8 us -> 26.2 us  [dispatch(): lax.all_to_all(send, 'ep', split_axis=0, concat_axis=0, tiled=True, axis_...]
    dot_general x2 -> x3, matrix products: 35.3 us -> 41.3 us  [experts(): jnp.dot(hidden, down_mat, preferred_element_type=jnp.float32)]
    all_to_all x2 -> x3, starting transfers between devices: 10.3 us -> 16 us  [dispatch(): lax.all_to_all(send, 'ep', split_axis=0, concat_axis=0, tiled=True, axis_...]
    concatenate x0 -> x1, other arithmetic: none -> 3.96 us  [on_device(): jnp.concatenate([early_results.reshape(half, cut, -1), late_results.resha...]
  transfers between devices with their start and end apart: 6 -> 8, of which waited for: 4 -> 5; matrix products, arithmetic and copies ran while one was open for 11% -> 27% of each run, Pallas kernels for 0% -> 0%
where the time goes in v3:
time: 286 us; the launch traced here: 284 us
  waiting for transfers between devices  155 us (54%)
  matrix products  81.8 us (29%)
  starting transfers between devices  33.6 us (12%)
  other arithmetic  10.2 us (4%)
  local copies, waits for them, and re-layouts  3.13 us (1%)
    all_to_all x2, waiting for transfers between devices, collect(): lax.all_to_all(results, 'ep', split_axis=0, concat_axis=0, tiled=True, ax...  70.8 us
    ppermute x1, waiting for transfers between devices, on_device(): far_plan = lax.ppermute(plan, 'ep', across)  46 us
    dot_general x3, matrix products, experts(): jnp.dot(hidden, down_mat, preferred_element_type=jnp.float32)  41.3 us
    all_to_all x3, waiting for transfers between devices, dispatch(): lax.all_to_all(send, 'ep', split_axis=0, concat_axis=0, tiled=True, axis_...  26.2 us
    dot_general x2, matrix products, experts(): gate_pre = jnp.dot(arrived, gate_mat, preferred_element_type=jnp.float32)  16.8 us
    all_to_all x3, starting transfers between devices, dispatch(): lax.all_to_all(send, 'ep', split_axis=0, concat_axis=0, tiled=True, axis_...  16 us
    ppermute x1, waiting for transfers between devices, on_device(): reply = lax.ppermute(reply.astype(jnp.bfloat16), 'ep', across)  11.9 us
    all_to_all x2, starting transfers between devices, collect(): lax.all_to_all(results, 'ep', split_axis=0, concat_axis=0, tiled=True, ax...  10.8 us
  transfers between devices with their start and end apart: 8, of which 5 were waited for; matrix products, arithmetic and copies ran while one was open for 27% of the time, Pallas kernels for 0%

profile of v3, /device:TPU:2, one launch (start us, length us, event | category | flops | bytes accessed | tf_op | source)
XLA Modules:
  0.0 283.8 jit_solution(8348810475842148207)
XLA Ops:
  9.7 5.3 %all-to-all-start = ((bf16[16,24,2048]{2,1,0:T(8,128)(2,1)}), bf16[16,24,2048]{2,1,0:T(8,128)(2,1)}, u32[]{:S(2)}, u32[]{:S(2)}) async-start(bf16[16,24,2048]{2,1,0:T(8,128)(2,1)} %bitcast.4), calls=%async_computation | async-start | bytes 3145728 | tf_op jit(solution)/shard_map/all_to_all | solution.py:53
  15.0 2.6 collective-permute-start
  18.1 46.0 %collective-permute-done.1 = f32[256,4]{0,1:T(4,128)S(1)} collective-permute-done((f32[256,4]{0,1:T(4,128)S(1)}, f32[256,4]{0,1:T(4,128)S(1)}, u32[]{:S(2)}, u32[]{:S(2)}) %collective-permute-start.1) | collective-permute-done | bytes 4128 | tf_op jit(solution)/shard_map/ppermute | solution.py:36
  64.1 2.7 convolution_convert_fusion
  66.8 4.7 %all-to-all-start.1 = ((bf16[16,48,2048]{2,1,0:T(8,128)(2,1)}), bf16[16,48,2048]{2,1,0:T(8,128)(2,1)}, u32[]{:S(2)}, u32[]{:S(2)}) async-start(bf16[16,48,2048]{2,1,0:T(8,128)(2,1)} %bitcast.8), calls=%async_computation.1 | async-start | bytes 6291456 | tf_op jit(solution)/shard_map/all_to_all | solution.py:53
  71.6 7.3 %fusion.10 = f32[384,1536]{1,0:T(8,128)} fusion(bf16[384,2048]{1,0:T(8,128)(2,1)} %bitcast.5, bf16[1,2048,1536]{2,1,0:T(8,128)(2,1)} %param.12), kind=kOutput, calls=%fused_computation.10 | convolution fusion | flops 2415919104 | bytes 10223616 | tf_op jit(solution)/shard_map/dot_general | solution.py:59
  78.9 12.1 %fusion.29 = bf16[384,2048]{1,0:T(8,128)(2,1)} fusion(bf16[1,1536,2048]{2,1,0:T(8,128)(2,1)} %param.13, f32[384,1536]{1,0:T(8,128)} %fusion.10, bf16[384,2048]{1,0:T(8,128)(2,1)} %bitcast.5, bf16[1,2048,1536]{2,1,0:T(8,128)(2,1)} %param.11), kind=kOutput, calls=%fused_computation.24 | convolution fusion | flops 4836163584 | bytes 18087936 | tf_op jit(solution)/shard_map/dot_general | solution.py:61
  91.0 26.2 %all-to-all-done.1 = bf16[16,48,2048]{2,1,0:T(8,128)(2,1)} async-done(((bf16[16,48,2048]{2,1,0:T(8,128)(2,1)}), bf16[16,48,2048]{2,1,0:T(8,128)(2,1)}, u32[]{:S(2)}, u32[]{:S(2)}) %all-to-all-start.1) | async-done | bytes 3145760 | tf_op jit(solution)/shard_map/all_to_all | solution.py:53
  117.2 1.8 convolution_convert_fusion.1
  119.1 6.1 %all-to-all-start.2 = ((bf16[16,24,2048]{2,1,0:T(8,128)(2,1)}), bf16[16,24,2048]{2,1,0:T(8,128)(2,1)S(1)}, u32[]{:S(2)}, u32[]{:S(2)}) async-start(bf16[16,24,2048]{2,1,0:T(8,128)(2,1)} %bitcast.13), calls=%async_computation.2 | async-start | bytes 3145728 | tf_op jit(solution)/shard_map/all_to_all | solution.py:53
  125.1 9.5 %fusion.14 = f32[768,1536]{1,0:T(8,128)} fusion(bf16[768,2048]{1,0:T(8,128)(2,1)} %bitcast.9, bf16[1,2048,1536]{2,1,0:T(8,128)(2,1)} %param.11), kind=kOutput, calls=%fused_computation.14 | convolution fusion | flops 4831838208 | bytes 14155776 | tf_op jit(solution)/shard_map/dot_general | solution.py:58
  134.6 17.2 %fusion.20 = bf16[768,2048]{1,0:T(8,128)(2,1)} fusion(bf16[1,1536,2048]{2,1,0:T(8,128)(2,1)} %param.13, f32[768,1536]{1,0:T(8,128)} %fusion.14, bf16[768,2048]{1,0:T(8,128)(2,1)} %bitcast.9, bf16[1,2048,1536]{2,1,0:T(8,128)(2,1)} %param.12), kind=kOutput, calls=%fused_computation.20 | convolution fusion | flops 9672327168 | bytes 23592960 | tf_op jit(solution)/shard_map/dot_general | solution.py:61
  153.1 5.1 %all-to-all-start.3 = ((bf16[16,48,2048]{2,1,0:T(8,128)(2,1)}), bf16[16,48,2048]{2,1,0:T(8,128)(2,1)S(1)}, u32[]{:S(2)}, u32[]{:S(2)}) async-start(bf16[16,48,2048]{2,1,0:T(8,128)(2,1)} %bitcast.96), calls=%async_computation.3 | async-start | bytes 6291456 | tf_op jit(solution)/shard_map/all_to_all | solution.py:64
  158.2 7.3 %fusion.12 = f32[384,1536]{1,0:T(8,128)} fusion(bf16[384,2048]{1,0:T(8,128)(2,1)} %bitcast.97, bf16[1,2048,1536]{2,1,0:T(8,128)(2,1)} %param.11), kind=kOutput, calls=%fused_computation.12 | convolution fusion | flops 2415919104 | bytes 10223616 | tf_op jit(solution)/shard_map/dot_general | solution.py:58
  165.5 12.0 %fusion.32 = bf16[384,2048]{1,0:T(8,128)(2,1)} fusion(bf16[1,1536,2048]{2,1,0:T(8,128)(2,1)} %param.13, bf16[384,2048]{1,0:T(8,128)(2,1)} %bitcast.98, bf16[1,2048,1536]{2,1,0:T(8,128)(2,1)} %param.12, f32[384,1536]{1,0:T(8,128)} %fusion.12), kind=kOutput, calls=%fused_computation.25 | convolution fusion | flops 4836163584 | bytes 18087936 | tf_op jit(solution)/shard_map/dot_general | solution.py:61
  177.5 4.0 %pad_maximum_fusion = bf16[16,48,2048]{2,1,0:T(8,128)(2,1)} fusion(bf16[16,24,2048]{2,1,0:T(8,128)(2,1)} %bitcast.100, bf16[16,24,2048]{2,1,0:T(8,128)(2,1)} %bitcast.99), kind=kLoop, calls=%fused_computation.21 | loop fusion | flops 6291456 | bytes 6291456 | tf_op jit(solution)/shard_map/concatenate | solution.py:87
  181.4 23.5 %all-to-all-done.3 = bf16[16,48,2048]{2,1,0:T(8,128)(2,1)S(1)} async-done(((bf16[16,48,2048]{2,1,0:T(8,128)(2,1)}), bf16[16,48,2048]{2,1,0:T(8,128)(2,1)S(1)}, u32[]{:S(2)}, u32[]{:S(2)}) %all-to-all-start.3) | async-done | bytes 3145760 | tf_op jit(solution)/shard_map/all_to_all | solution.py:64
  204.9 5.7 %all-to-all-start.4 = ((bf16[16,48,2048]{2,1,0:T(8,128)(2,1)}), bf16[16,48,2048]{2,1,0:T(8,128)(2,1)}, u32[]{:S(2)}, u32[]{:S(2)}) async-start(bf16[16,48,2048]{2,1,0:T(8,128)(2,1)} %pad_maximum_fusion), calls=%async_computation.4 | async-start | bytes 6291456 | tf_op jit(solution)/shard_map/all_to_all | solution.py:64
  211.7 2.1 fusion.37
  213.8 3.8 %collective-permute-start.2 = (bf16[256,2048]{1,0:T(8,128)(2,1)}, bf16[256,2048]{1,0:T(8,128)(2,1)S(1)}, u32[]{:S(2)}, u32[]{:S(2)}) collective-permute-start(bf16[256,2048]{1,0:T(8,128)(2,1)} %fusion.37), channel_id=1, source_target_pairs={{0,16},{1,17},{2,18},{3,19},{4,20},{5,21},{6,22},{7,23},{8,24},{9,... | collective-permute-start | bytes 3145736 | tf_op jit(solution)/shard_map/ppermute | solution.py:97
  217.6 47.3 %all-to-all-done.4 = bf16[16,48,2048]{2,1,0:T(8,128)(2,1)} async-done(((bf16[16,48,2048]{2,1,0:T(8,128)(2,1)}), bf16[16,48,2048]{2,1,0:T(8,128)(2,1)}, u32[]{:S(2)}, u32[]{:S(2)}) %all-to-all-start.4) | async-done | bytes 3145760 | tf_op jit(solution)/shard_map/all_to_all | solution.py:64
  264.9 2.9 %convolution_multiply_fusion.3 = f32[256,2048]{1,0:T(8,128)S(1)} fusion(bf16[768,2048]{1,0:T(8,128)(2,1)} %bitcast.21, f32[256]{0:T(256)S(1)} %bitcast.113, s32[256]{0:T(256)S(1)} %bitcast.110), kind=kOutput, calls=%fused_computation.33 | convolution fusion | flops 806027264 | bytes 5244928 | tf_op jit(solution)/shard_map/dot_general | solution.py:71
  267.8 11.9 %collective-permute-done.2 = bf16[256,2048]{1,0:T(8,128)(2,1)S(1)} collective-permute-done((bf16[256,2048]{1,0:T(8,128)(2,1)}, bf16[256,2048]{1,0:T(8,128)(2,1)S(1)}, u32[]{:S(2)}, u32[]{:S(2)}) %collective-permute-start.2) | collective-permute-done | bytes 1048608 | tf_op jit(solution)/shard_map/ppermute | solution.py:97
  279.7 4.1 %add_convert_fusion = bf16[256,2048]{1,0:T(8,128)(2,1)} fusion(bf16[256,2048]{1,0:T(8,128)(2,1)S(1)} %collective-permute-done.2, f32[256]{0:T(256)S(1)} %broadcast_select_fusion, f32[256,2048]{1,0:T(8,128)S(1)} %convolution_multiply_fusion.3, bf16[768,2048]{1,0:T(8,128)(2,1)} %bitcast.21, f32[256]{0:T(256)S(1)} %bitcast.106, s32[256]{0:T(256)S(1)} %bitcast.103), kind=kOutput, calls=%fused_computation.41 | convolution fusion | flops 808648704 | bytes 7343104 | tf_op jit(solution)/shard_map/dot_general | solution.py:71
  (46 shorter events, 12.6 us)
Async XLA Ops:
  0.0 6.9 %copy-start = (bf16[256,2048]{1,0:T(8,128)(2,1)S(1)}, bf16[256,2048]{1,0:T(8,128)(2,1)}, u32[]{:S(2)}) copy-start(bf16[256,2048]{1,0:T(8,128)(2,1)} %param.7) | copy-start | bytes 3145732
  7.9 9.7 %copy-start.2 = (s32[256,2]{0,1:T(2,128)S(1)}, s32[256,2]{0,1:T(2,128)}, u32[]{:S(2)}) copy-start(s32[256,2]{0,1:T(2,128)} %param.9) | copy-start | bytes 6148
  9.7 54.4 %all-to-all-start = ((bf16[16,24,2048]{2,1,0:T(8,128)(2,1)}), bf16[16,24,2048]{2,1,0:T(8,128)(2,1)}, u32[]{:S(2)}, u32[]{:S(2)}) async-start(bf16[16,24,2048]{2,1,0:T(8,128)(2,1)} %bitcast.4), calls=%async_computation | async-start | bytes 3145728 | tf_op jit(solution)/shard_map/all_to_all | solution.py:53
  15.0 49.1 %collective-permute-start = (bf16[256,2048]{1,0:T(8,128)(2,1)S(1)}, bf16[256,2048]{1,0:T(8,128)(2,1)S(1)}, u32[]{:S(2)}, u32[]{:S(2)}) collective-permute-start(bf16[256,2048]{1,0:T(8,128)(2,1)S(1)} %fusion.40), channel_id=1, source_target_pairs={{0,16},{1,17},{2,18},{3,19},{4,20},{5,21},{6,22},{7,23},{8,24},{9,... | collective-permute-start | bytes 3145736 | tf_op jit(solution)/shard_map/ppermute | solution.py:27
  17.6 46.5 %collective-permute-start.1 = (f32[256,4]{0,1:T(4,128)S(1)}, f32[256,4]{0,1:T(4,128)S(1)}, u32[]{:S(2)}, u32[]{:S(2)}) collective-permute-start(f32[256,4]{0,1:T(4,128)S(1)} %pad_maximum_fusion.1), channel_id=1, source_target_pairs={{0,16},{1,17},{2,18},{3,19},{4,20},{5,21},{6,22},{7,23},{8,24},{9,... | collective-permute-start | bytes 12296 | tf_op jit(solution)/shard_map/ppermute | solution.py:36
  66.8 50.4 %all-to-all-start.1 = ((bf16[16,48,2048]{2,1,0:T(8,128)(2,1)}), bf16[16,48,2048]{2,1,0:T(8,128)(2,1)}, u32[]{:S(2)}, u32[]{:S(2)}) async-start(bf16[16,48,2048]{2,1,0:T(8,128)(2,1)} %bitcast.8), calls=%async_computation.1 | async-start | bytes 6291456 | tf_op jit(solution)/shard_map/all_to_all | solution.py:53
  119.1 32.8 %all-to-all-start.2 = ((bf16[16,24,2048]{2,1,0:T(8,128)(2,1)}), bf16[16,24,2048]{2,1,0:T(8,128)(2,1)S(1)}, u32[]{:S(2)}, u32[]{:S(2)}) async-start(bf16[16,24,2048]{2,1,0:T(8,128)(2,1)} %bitcast.13), calls=%async_computation.2 | async-start | bytes 3145728 | tf_op jit(solution)/shard_map/all_to_all | solution.py:53
  151.9 1.2 copy-start.1
  153.1 51.8 %all-to-all-start.3 = ((bf16[16,48,2048]{2,1,0:T(8,128)(2,1)}), bf16[16,48,2048]{2,1,0:T(8,128)(2,1)S(1)}, u32[]{:S(2)}, u32[]{:S(2)}) async-start(bf16[16,48,2048]{2,1,0:T(8,128)(2,1)} %bitcast.96), calls=%async_computation.3 | async-start | bytes 6291456 | tf_op jit(solution)/shard_map/all_to_all | solution.py:64
  204.9 60.0 %all-to-all-start.4 = ((bf16[16,48,2048]{2,1,0:T(8,128)(2,1)}), bf16[16,48,2048]{2,1,0:T(8,128)(2,1)}, u32[]{:S(2)}, u32[]{:S(2)}) async-start(bf16[16,48,2048]{2,1,0:T(8,128)(2,1)} %pad_maximum_fusion), calls=%async_computation.4 | async-start | bytes 6291456 | tf_op jit(solution)/shard_map/all_to_all | solution.py:64
  213.8 65.9 %collective-permute-start.2 = (bf16[256,2048]{1,0:T(8,128)(2,1)}, bf16[256,2048]{1,0:T(8,128)(2,1)S(1)}, u32[]{:S(2)}, u32[]{:S(2)}) collective-permute-start(bf16[256,2048]{1,0:T(8,128)(2,1)} %fusion.37), channel_id=1, source_target_pairs={{0,16},{1,17},{2,18},{3,19},{4,20},{5,21},{6,22},{7,23},{8,24},{9,... | collective-permute-start | bytes 3145736 | tf_op jit(solution)/shard_map/ppermute | solution.py:97
